TPU v7x, 128 devices: a whole 4x4x4 slice. The times are simulated.
128 devices in a mesh: rep: 2 (over z_hi), fs: 32 (over z_lo, y, x), tp: 2 (over core).
Axes of the slice: x: 4, y: 4, z: 4 (z_hi: 2, z_lo: 2; z = z_hi * 2 + z_lo), core: 2. Of those that a mesh axis runs over, the one named last changes fastest.
Arguments:
- tokens: bfloat16 [49152, 2048], P(('rep', 'fs', 'tp')), may hold values from -6 to 6
- outer_weight: float32 [2048, 1536], P('fs', 'tp'), may hold values from -0.125 to 0.125
- inner_weight: float32 [2048, 1536], P('fs', 'tp'), may hold values from -0.125 to 0.125
- value_weight: float32 [2048, 1536], P('fs', 'tp'), may hold values from -0.125 to 0.125
- conv_taps: float32 [3, 1536], P(None, 'tp'), may hold values from -3 to 3
- mix_out: float32 [1536, 2048], P('tp', 'fs'), may hold values from -0.15625 to 0.15625
- norm_first: float32 [2048], replicated, may hold values from 0.1 to 1.9
- up_weight: float32 [2048, 4096], P('fs', 'tp'), may hold values from -0.125 to 0.125
- down_weight: float32 [4096, 2048], P('tp', 'fs'), may hold values from -0.09375 to 0.09375
- norm_second: float32 [2048], replicated, may hold values from 0.1 to 1.9
Outputs:
- encoded: bfloat16 [49152, 2048], P(('rep', 'fs', 'tp'))
All inputs are finite; a program needn't handle non-finite values.
Results may differ from a plain program's by a relative error of at most 0.015.
Values may be sent and summed in bfloat16 or wider, within the bound.
No kernel may reach another device: no remote copies, remote signals or barrier semaphores. Data moves between devices by JAX's collectives and lax.ppermute only.
A program may use at most 128 MiB of HBM per device.

v0:
```python
import jax
import jax.numpy as jnp
from jax import lax
from jax.sharding import Mesh
from jax.sharding import PartitionSpec as P

SEQ = 128
FS = ("fs_0", "fs_1", "fs_2")
REP_FS_TP = ("rep", "fs_0", "fs_1", "fs_2", "tp")
residual_scale = 2.0**0.25
norm_epsilon = 1e-05


def in_one_piece(arrays, axis, dim, along):
    ends, at = ([], 0)
    for a in arrays[:-1]:
        at += a.shape[along]
        ends.append(at)
    both = jnp.concatenate(arrays, axis=along)
    return tuple(jnp.split(lax.all_gather(both, axis, axis=dim, tiled=True), ends, axis=along))


def laid_out(tiles, dim):
    tiles = jnp.moveaxis(tiles, 0, dim)
    lengths = tiles.shape
    return tiles.reshape(*lengths[:dim], lengths[dim] * lengths[dim + 1], *lengths[dim + 2 :])


def stacked_from(x, axes, order):
    tiles = x
    for k in order:
        tiles = lax.all_gather(tiles, axes[k])
    done = order[::-1]
    back = [done.index(k) for k in range(len(axes))]
    tiles = tiles.transpose(*back, *range(len(axes), tiles.ndim))
    return tiles.reshape(-1, *x.shape)


def whole_of(x, axes, order, dim):
    return laid_out(stacked_from(x, axes, order), dim)


def cut_along(x, dim, length):
    before, after = (x.shape[:dim], x.shape[dim + 1 :])
    return jnp.moveaxis(x.reshape(*before, length, -1, *after), dim, 0)


def sum_at_owner(x, axis, dim):
    tiles = cut_along(x, dim, lax.axis_size(axis))
    arrived = lax.all_to_all(tiles, axis, split_axis=0, concat_axis=0, tiled=True)
    return arrived.astype(jnp.float32).sum(axis=0)


def layer_norm(values, scaling):
    center = values - jnp.mean(values, axis=-1, keepdims=True)
    spread = jnp.mean(center * center, axis=-1, keepdims=True)
    return center * lax.rsqrt(spread + norm_epsilon) * scaling


def short_conv(product, conv_taps):
    places = jnp.arange(product.shape[0], dtype=jnp.int32) % SEQ
    blank = jnp.zeros((1, product.shape[1]), jnp.float32)
    before = jnp.concatenate([blank, product[:-1]], axis=0)
    after = jnp.concatenate([product[1:], blank], axis=0)
    before = jnp.where((places > 0)[:, None], before, 0.0)
    after = jnp.where((places < SEQ - 1)[:, None], after, 0.0)
    return conv_taps[0] * before + conv_taps[1] * product + conv_taps[2] * after


def local(
    tokens,
    outer_weight,
    inner_weight,
    value_weight,
    conv_taps,
    mix_out,
    norm_first,
    up_weight,
    down_weight,
    norm_second,
):
    grouped = lax.all_gather(tokens, "tp", axis=0, tiled=True)
    outer_bf = outer_weight.astype(jnp.bfloat16)
    inner_bf = inner_weight.astype(jnp.bfloat16)
    value_bf = value_weight.astype(jnp.bfloat16)
    outer_full, inner_full, value_full = in_one_piece((outer_bf, inner_bf, value_bf), FS, 0, 1)
    outer = jnp.dot(grouped, outer_full, preferred_element_type=jnp.float32)
    inner = jnp.dot(grouped, inner_full, preferred_element_type=jnp.float32)
    value = jnp.dot(grouped, value_full, preferred_element_type=jnp.float32)
    mixed = (outer * short_conv(inner * value, conv_taps)).astype(jnp.bfloat16)
    mixout_full = whole_of(mix_out.astype(jnp.bfloat16), FS, (0, 1, 2), 1)
    selected = mixed
    mixing = sum_at_owner(
        jnp.dot(selected, mixout_full, preferred_element_type=jnp.float32).astype(jnp.bfloat16),
        "tp",
        0,
    )
    first = layer_norm(residual_scale * tokens.astype(jnp.float32) + mixing, norm_first).astype(
        jnp.bfloat16
    )
    grouped_first = lax.all_gather(first, "tp", axis=0, tiled=True)
    upward_bf = up_weight.astype(jnp.bfloat16)
    upward_full = lax.all_gather(upward_bf, FS, axis=0, tiled=True)
    raised = jnp.dot(grouped_first, upward_full, preferred_element_type=jnp.float32)
    raised = jax.nn.relu(raised)
    hidden = (raised * raised).astype(jnp.bfloat16)
    down_full = lax.all_gather(down_weight.astype(jnp.bfloat16), FS, axis=1, tiled=True)
    selected = hidden
    lowered = sum_at_owner(
        jnp.dot(selected, down_full, preferred_element_type=jnp.float32).astype(jnp.bfloat16),
        "tp",
        0,
    )
    return layer_norm(residual_scale * first.astype(jnp.float32) + lowered, norm_second).astype(
        jnp.bfloat16
    )


def solution(mesh):
    finer = Mesh(
        mesh.devices.reshape(mesh.shape["rep"], 2, 4, 4, mesh.shape["tp"]),
        ("rep", "fs_0", "fs_1", "fs_2", "tp"),
    )
    placed = (
        P(REP_FS_TP, None),
        P(FS, "tp"),
        P(FS, "tp"),
        P(FS, "tp"),
        P(None, "tp"),
        P("tp", FS),
        P(),
        P(FS, "tp"),
        P("tp", FS),
        P(),
    )
    return jax.shard_map(
        local, mesh=finer, in_specs=placed, out_specs=P(REP_FS_TP, None), check_vma=False
    )
```

profile of v0, /device:TPU:1, one launch (start us, length us, event | category | flops | bytes accessed | tf_op | source)
XLA Modules:
  0.0 637.7 jit_solution(7984287710747323062)
XLA Ops:
  6.5 0.0 all-gather.20.cloned.1.call-start
  6.6 1.0 convert_element_type.53
  7.6 5.6 all-gather
  13.2 0.0 copy-start.9
  13.3 13.2 %all-gather.1 = bf16[8,768,64]{1,2,0:T(8,128)(2,1)} all-gather(bf16[2,768,64]{1,2,0:T(8,128)(2,1)S(1)} %bitcast.37), channel_id=3, replica_groups=mesh['rep'=2,'fs_0'=2,'fs_1'=4,'fs_2'=4,'tp'=2] {'fs_1'}, dimensions={0}, use_global_device_ids=true | all-gather | bytes 983040 | tf_op jit(solution)/shard_map/all_gather | solution.py:32
  26.5 0.0 all-gather.20.cloned.1.call-update
  26.5 0.0 all-gather.12.cloned.1.call-start
  26.6 0.7 all-gather.12.cloned.1.call-update
  27.3 0.0 all-gather.10.cloned.1.call-start
  27.3 0.0 copy-done.4
  27.3 0.0 copy-done.5
  27.4 0.7 pad_maximum_fusion
  28.1 0.0 all-gather.10.cloned.1.call-update
  28.2 0.0 all-gather.16.cloned.1.call-start
  28.2 0.7 convert_element_type.58
  29.0 0.0 all-gather.16.cloned.1.call-update
  29.0 0.0 all-gather.14.cloned.1.call-start
  29.0 0.0 copy-done.9
  29.1 41.1 %all-gather.20.cloned.1.call-done = bf16[16,2,768,64]{2,3,1,0:T(8,128)(2,1)} async-done(((bf16[4,2,768,64]{2,3,1,0:T(8,128)(2,1)}), bf16[16,2,768,64]{2,3,1,0:T(8,128)(2,1)}) %all-gather.20.cloned.1.call-update) | async-done | bytes 3145744 | tf_op jit(solution)/shard_map/all_gather | solution.py:32
  70.2 3.9 copy.15
  74.1 13.4 %all-gather.12.cloned.1.call-done = bf16[768,2048]{1,0:T(8,128)(2,1)} async-done(((bf16[384,2048]{1,0:T(8,128)(2,1)}), bf16[768,2048]{1,0:T(8,128)(2,1)}) %all-gather.12.cloned.1.call-update) | async-done | bytes 3145744 | tf_op jit(solution)/shard_map/all_gather | solution.py:82
  87.5 149.6 %all-gather.10.cloned.1.call-done = bf16[2048,2304]{1,0:T(8,128)(2,1)} async-done(((bf16[64,2304]{1,0:T(8,128)(2,1)}), bf16[2048,2304]{1,0:T(8,128)(2,1)}) %all-gather.10.cloned.1.call-update) | async-done | bytes 9437200 | tf_op jit(solution)/shard_map/all_gather | solution.py:20
  237.1 5.6 fusion
  242.8 4.6 multiply_bitcast_fusion
  247.3 2.9 fusion.21
  250.3 13.9 %convolution_convert_fusion.1 = bf16[768,2048]{1,0:T(8,128)(2,1)} fusion(bf16[768,2048]{0,1:T(8,128)(2,1)} %bitcast.32, f32[767,768]{0,1:T(8,128)} %get-tuple-element.9, f32[768,768]{0,1:T(8,128)S(1)} %multiply_bitcast_fusion, f32[767,768]{0,1:T(8,128)} %get-tuple-element.8, bf16[768,2048]{1,0:T(8,128)(2,1)} %all-gather.12.cloned.1.call-done, ...), kind=kOutput, calls=%fused_computation.4 | convolution fusion | flops 4838719488 | bytes 19671552 | tf_op jit(solution)/shard_map/dot_general | solution.py:94
  264.2 28.7 %all_to_all.10 = bf16[2,384,2048]{2,1,0:T(8,128)(2,1)S(1)} all-to-all(bf16[2,384,2048]{2,1,0:T(8,128)(2,1)} %bitcast.33), channel_id=1, replica_groups=mesh['rep'=2,'fs_0'=2,'fs_1'=4,'fs_2'=4,'tp'=2] {'tp'}, dimensions={0} | all-to-all | bytes 6291456 | tf_op jit(solution)/shard_map/all_to_all | solution.py:50
  292.8 0.7 convert_reduce_fusion.1
  293.6 0.7 copy-done.1
  294.2 0.5 fusion.11
  294.7 0.7 multiply_reduce_fusion.1
  295.5 0.0 copy-start.3
  295.5 1.8 multiply_convert_fusion.2
  297.3 0.0 all-gather.14.cloned.1.call-update
  297.3 0.0 all-gather.18.cloned.1.call-start
  297.4 0.8 convert_element_type.60
  298.2 0.0 all-gather.18.cloned.1.call-update
  298.2 106.1 %all-gather.16.cloned.1.call-done = bf16[2048,2048]{1,0:T(8,128)(2,1)} async-done(((bf16[64,2048]{1,0:T(8,128)(2,1)}), bf16[2048,2048]{1,0:T(8,128)(2,1)}) %all-gather.16.cloned.1.call-update) | async-done | bytes 8388624 | tf_op jit(solution)/shard_map/all_gather | solution.py:103
  404.2 37.8 %all-gather.14.cloned.1.call-done = bf16[768,2048]{1,0:T(8,128)(2,1)} async-done(((bf16[384,2048]{1,0:T(8,128)(2,1)}), bf16[768,2048]{1,0:T(8,128)(2,1)}) %all-gather.14.cloned.1.call-update) | async-done | bytes 3145744 | tf_op jit(solution)/shard_map/all_gather | solution.py:101
  442.1 10.0 %multiply_convert_fusion = bf16[768,2048]{1,0:T(8,128)(2,1)S(1)} fusion(bf16[768,2048]{1,0:T(8,128)(2,1)} %all-gather.14.cloned.1.call-done, bf16[2048,2048]{1,0:T(8,128)(2,1)} %all-gather.16.cloned.1.call-done), kind=kOutput, calls=%fused_computation.1 | convolution fusion | flops 6447169536 | bytes 14680064 | tf_op jit(solution)/shard_map/dot_general | solution.py:104
  452.1 138.3 %all-gather.18.cloned.1.call-done = bf16[2048,2048]{0,1:T(8,128)(2,1)} async-done(((bf16[2048,64]{0,1:T(8,128)(2,1)}), bf16[2048,2048]{0,1:T(8,128)(2,1)}) %all-gather.18.cloned.1.call-update) | async-done | bytes 8388624 | tf_op jit(solution)/shard_map/all_gather | solution.py:107
  590.4 9.1 %convolution_convert_fusion = bf16[768,2048]{1,0:T(8,128)(2,1)S(1)} fusion(bf16[768,2048]{1,0:T(8,128)(2,1)S(1)} %multiply_convert_fusion, bf16[2048,2048]{0,1:T(8,128)(2,1)} %all-gather.18.cloned.1.call-done), kind=kOutput, calls=%fused_computation.3 | convolution fusion | flops 6444023808 | bytes 14680064 | tf_op jit(solution)/shard_map/dot_general | solution.py:110
  599.5 26.9 %all_to_all.11 = bf16[2,384,2048]{2,1,0:T(8,128)(2,1)S(1)} all-to-all(bf16[2,384,2048]{2,1,0:T(8,128)(2,1)S(1)} %bitcast.34), channel_id=1, replica_groups=mesh['rep'=2,'fs_0'=2,'fs_1'=4,'fs_2'=4,'tp'=2] {'tp'}, dimensions={0} | all-to-all | bytes 6291456 | tf_op jit(solution)/shard_map/all_to_all | solution.py:50
  626.4 0.7 convert_reduce_fusion
  627.2 0.7 copy-done
  627.8 0.5 fusion.12
  628.3 0.7 multiply_reduce_fusion
  629.1 1.8 multiply_convert_fusion.1
  (25 shorter events, 0.1 us)
Async XLA Ops:
  6.5 20.8 %copy-start.4 = (f32[64,768]{1,0:T(8,128)S(1)}, f32[64,768]{1,0:T(8,128)}, u32[]{:S(2)}) copy-start(f32[64,768]{1,0:T(8,128)} %param.11) | copy-start | bytes 589828
  6.5 20.8 %copy-start.5 = (f32[64,768]{1,0:T(8,128)S(1)}, f32[64,768]{1,0:T(8,128)}, u32[]{:S(2)}) copy-start(f32[64,768]{1,0:T(8,128)} %param.12) | copy-start | bytes 589828
  6.5 20.8 %copy-start.6 = (f32[64,768]{1,0:T(8,128)S(1)}, f32[64,768]{1,0:T(8,128)}, u32[]{:S(2)}) copy-start(f32[64,768]{1,0:T(8,128)} %param.13) | copy-start | bytes 589828
  6.5 21.7 %copy-start.2 = (f32[64,2048]{1,0:T(8,128)S(1)}, f32[64,2048]{1,0:T(8,128)}, u32[]{:S(2)}) copy-start(f32[64,2048]{1,0:T(8,128)} %param.17) | copy-start | bytes 1572868
  6.5 63.7 %all-gather.20.cloned.1.call-start = ((), (), s32[]{:S(2)}) async-start(), calls=%async_computation.7 | async-start | bytes 3932160 | tf_op jit(solution)/shard_map/all_gather | solution.py:32
  13.2 15.8 %copy-start.9 = (f32[3,768]{1,0:T(4,128)S(1)}, f32[3,768]{1,0:T(4,128)}, u32[]{:S(2)}) copy-start(f32[3,768]{1,0:T(4,128)} %param.14) | copy-start | bytes 27652
  26.5 61.0 %all-gather.12.cloned.1.call-start = ((), (), s32[]{:S(2)}) async-start(), calls=%async_computation.3 | async-start | bytes 4718592 | tf_op jit(solution)/shard_map/all_gather | solution.py:82
  27.3 209.8 %all-gather.10.cloned.1.call-start = ((), (), s32[]{:S(2)}) async-start(), calls=%async_computation.2 | async-start | bytes 9732096 | tf_op jit(solution)/shard_map/all_gather | solution.py:20
  28.2 376.1 %all-gather.16.cloned.1.call-start = ((), (), s32[]{:S(2)}) async-start(), calls=%async_computation.5 | async-start | bytes 8650752 | tf_op jit(solution)/shard_map/all_gather | solution.py:103
  29.0 413.1 %all-gather.14.cloned.1.call-start = ((), (), s32[]{:S(2)}) async-start(), calls=%async_computation.4 | async-start | bytes 4718592 | tf_op jit(solution)/shard_map/all_gather | solution.py:101
  237.1 5.7 copy-start.10
  292.8 1.4 copy-start.1
  294.7 0.7 copy-start.7
  295.5 1.9 copy-start.3
  297.3 293.0 %all-gather.18.cloned.1.call-start = ((), (), s32[]{:S(2)}) async-start(), calls=%async_computation.6 | async-start | bytes 8650752 | tf_op jit(solution)/shard_map/all_gather | solution.py:107
  626.4 1.4 copy-start
  628.3 0.7 copy-start.8
Sparse Core Ops, SparseCore 0:
  26.6 43.5 all-gather.19
  71.9 15.6 all-gather.11
  89.2 147.8 all-gather.9
  238.6 165.6 all-gather.15
  405.7 36.2 all-gather.13
  443.6 146.7 all-gather.17
where the time goes:
time: 638 us
  waiting for transfers between devices  487 us (76%)
  blocking collectives  74.4 us (12%)
  matrix products  43.3 us (7%)
  between operations  13.7 us (2%)
  other arithmetic  10.8 us (2%)
  local copies, waits for them, and re-layouts  8.27 us (1%)
    all_gather x1, waiting for transfers between devices, in_one_piece(): lax.all_gather(both, axis, axis=dim, tiled=True)  150 us
    all_gather x1, waiting for transfers between devices, local(): lax.all_gather(down_weight.astype(jnp.bfloat16), FS, axis=1, tiled=True)  138 us
    all_gather x1, waiting for transfers between devices, local(): upward_full = lax.all_gather(upward_bf, FS, axis=0, tiled=True)  106 us
    all_to_all x2, blocking collectives, sum_at_owner(): lax.all_to_all(tiles, axis, split_axis=0, concat_axis=0, tiled=True)  55.6 us
    all_gather x1, waiting for transfers between devices, stacked_from(): tiles = lax.all_gather(tiles, axes[k])  41.1 us
    all_gather x1, waiting for transfers between devices, local(): grouped_first = lax.all_gather(first, 'tp', axis=0, tiled=True)  37.8 us
    all_gather x2, blocking collectives, stacked_from(): tiles = lax.all_gather(tiles, axes[k])  18.8 us
    dot_general x1, matrix products, local(): jnp.dot(selected, mixout_full, preferred_element_type=jnp.float32)  13.9 us
  transfers between devices with their start and end apart: 6, of which 6 were waited for; matrix products, arithmetic and copies ran while one was open for 7% of the time, Pallas kernels for 0%

commit v1 on v0

--- a/solution.py
+++ b/solution.py
@@ -9,6 +9,13 @@
 REP_FS_TP = ("rep", "fs_0", "fs_1", "fs_2", "tp")
 residual_scale = 2.0**0.25
 norm_epsilon = 1e-05
+
+
+def gather_over(shard, mesh_axis, d):
+    devices = lax.axis_size(mesh_axis)
+    tiles = jnp.stack([shard for _ in range(devices)])
+    tiles = lax.all_to_all(tiles, mesh_axis, split_axis=0, concat_axis=0)
+    return jnp.concatenate(tiles, axis=d)
 
 
 def in_one_piece(arrays, axis, dim, along):
@@ -104,7 +111,7 @@
     raised = jnp.dot(grouped_first, upward_full, preferred_element_type=jnp.float32)
     raised = jax.nn.relu(raised)
     hidden = (raised * raised).astype(jnp.bfloat16)
-    down_full = lax.all_gather(down_weight.astype(jnp.bfloat16), FS, axis=1, tiled=True)
+    down_full = gather_over(down_weight.astype(jnp.bfloat16), FS, 1)
     selected = hidden
     lowered = sum_at_owner(
         jnp.dot(selected, down_full, preferred_element_type=jnp.float32).astype(jnp.bfloat16),

time: 638 us -> 559 us (0.88)
  waiting for transfers between devices: 487 us -> 414 us
  blocking collectives: 74.4 us -> 56.6 us
  starting transfers between devices: 0.24 us -> 6.66 us
    all_gather x1 -> x0, waiting for transfers between devices: 138 us -> none  [local(): lax.all_gather(down_weight.astype(jnp.bfloat16), FS, axis=1, tiled=True)]
    all_gather x1, waiting for transfers between devices: 106 us -> 176 us  [local(): upward_full = lax.all_gather(upward_bf, FS, axis=0, tiled=True)]
    all_to_all x2, blocking collectives: 55.6 us -> 37.6 us  [sum_at_owner(): lax.all_to_all(tiles, axis, split_axis=0, concat_axis=0, tiled=True)]
    all_to_all x0 -> x1, starting transfers between devices: none -> 6.46 us  [gather_over(): tiles = lax.all_to_all(tiles, mesh_axis, split_axis=0, concat_axis=0)]
  transfers between devices with their start and end apart: 6 -> 6, of which waited for: 6 -> 5; matrix products, arithmetic and copies ran while one was open for 7% -> 9% of each run, Pallas kernels for 0% -> 0%
where the time goes in v1:
time: 559 us; the launch traced here: 558 us
  waiting for transfers between devices  414 us (74%)
  blocking collectives  56.6 us (10%)
  matrix products  43.3 us (8%)
  between operations  13.4 us (2%)
  other arithmetic  12.5 us (2%)
  local copies, waits for them, and re-layouts  11.9 us (2%)
  starting transfers between devices  6.66 us (1%)
    all_gather x1, waiting for transfers between devices, local(): upward_full = lax.all_gather(upward_bf, FS, axis=0, tiled=True)  176 us
    all_gather x1, waiting for transfers between devices, in_one_piece(): lax.all_gather(both, axis, axis=dim, tiled=True)  150 us
    all_gather x1, waiting for transfers between devices, stacked_from(): tiles = lax.all_gather(tiles, axes[k])  41.1 us
    all_to_all x2, blocking collectives, sum_at_owner(): lax.all_to_all(tiles, axis, split_axis=0, concat_axis=0, tiled=True)  37.6 us
    all_gather x1, waiting for transfers between devices, local(): grouped_first = lax.all_gather(first, 'tp', axis=0, tiled=True)  33 us
    all_gather x2, blocking collectives, stacked_from(): tiles = lax.all_gather(tiles, axes[k])  19 us
    dot_general x1, matrix products, local(): jnp.dot(selected, mixout_full, preferred_element_type=jnp.float32)  13.9 us
    all_gather x1, waiting for transfers between devices, local(): grouped = lax.all_gather(tokens, 'tp', axis=0, tiled=True)  13.4 us
  transfers between devices with their start and end apart: 6, of which 5 were waited for; matrix products, arithmetic and copies ran while one was open for 9% of the time, Pallas kernels for 0%

profile of v1, /device:TPU:1, one launch (start us, length us, event | category | flops | bytes accessed | tf_op | source)
XLA Modules:
  0.0 558.5 jit_solution(9543314783399947747)
XLA Ops:
  6.5 0.0 all-gather.17.cloned.1.call-start
  6.6 1.0 convert_element_type.53
  7.6 5.6 %all-gather = bf16[1536,64]{0,1:T(8,128)(2,1)S(1)} all-gather(bf16[768,64]{0,1:T(8,128)(2,1)S(1)} %convert_element_type.53), channel_id=2, replica_groups=mesh['rep'=2,'fs_0'=2,'fs_1'=4,'fs_2'=4,'tp'=2] {'fs_0'}, dimensions={0}, use_global_device_ids=true | all-gather | bytes 294912 | tf_op jit(solution)/shard_map/all_gather | solution.py:39
  13.2 0.0 copy-start.3
  13.3 13.4 %all-gather.1 = bf16[8,768,64]{1,2,0:T(8,128)(2,1)} all-gather(bf16[2,768,64]{1,2,0:T(8,128)(2,1)S(1)} %bitcast.40), channel_id=3, replica_groups=mesh['rep'=2,'fs_0'=2,'fs_1'=4,'fs_2'=4,'tp'=2] {'fs_1'}, dimensions={0}, use_global_device_ids=true | all-gather | bytes 983040 | tf_op jit(solution)/shard_map/all_gather | solution.py:39
  26.6 0.0 all-gather.17.cloned.1.call-update
  26.6 0.0 all-gather.11.cloned.1.call-start
  26.7 0.7 all-gather.11.cloned.1.call-update
  27.4 0.0 all-gather.9.cloned.1.call-start
  27.4 0.0 copy-done.4
  27.5 0.0 copy-done.5
  27.5 0.0 copy-done.6
  27.5 0.7 pad_maximum_fusion
  28.3 0.0 all-gather.9.cloned.1.call-update
  28.3 0.0 all-gather.15.cloned.1.call-start
  28.4 0.7 convert_element_type.58
  29.1 0.0 all-gather.15.cloned.1.call-update
  29.2 0.0 copy-done.9
  29.2 41.1 %all-gather.17.cloned.1.call-done = bf16[16,2,768,64]{2,3,1,0:T(8,128)(2,1)} async-done(((bf16[4,2,768,64]{2,3,1,0:T(8,128)(2,1)}), bf16[16,2,768,64]{2,3,1,0:T(8,128)(2,1)}) %all-gather.17.cloned.1.call-update) | async-done | bytes 3145744 | tf_op jit(solution)/shard_map/all_gather | solution.py:39
  70.4 3.9 copy.16
  74.3 13.4 %all-gather.11.cloned.1.call-done = bf16[768,2048]{1,0:T(8,128)(2,1)} async-done(((bf16[384,2048]{1,0:T(8,128)(2,1)}), bf16[768,2048]{1,0:T(8,128)(2,1)}) %all-gather.11.cloned.1.call-update) | async-done | bytes 3145744 | tf_op jit(solution)/shard_map/all_gather | solution.py:89
  87.7 149.6 %all-gather.9.cloned.1.call-done = bf16[2048,2304]{1,0:T(8,128)(2,1)} async-done(((bf16[64,2304]{1,0:T(8,128)(2,1)}), bf16[2048,2304]{1,0:T(8,128)(2,1)}) %all-gather.9.cloned.1.call-update) | async-done | bytes 9437200 | tf_op jit(solution)/shard_map/all_gather | solution.py:27
  237.2 5.6 %fusion = f32[768,768]{1,0:T(8,128)S(1)} fusion(bf16[768,2048]{1,0:T(8,128)(2,1)} %all-gather.11.cloned.1.call-done, bf16[2048,2304]{1,0:T(8,128)(2,1)} %all-gather.9.cloned.1.call-done), kind=kOutput, calls=%fused_computation.5 | convolution fusion | flops 2415919104 | bytes 8650752 | tf_op jit(solution)/shard_map/dot_general | solution.py:96
  242.9 0.0 copy-done.10
  242.9 4.6 multiply_bitcast_fusion
  247.5 2.9 fusion.21
  250.4 13.9 %convolution_convert_fusion.1 = bf16[768,2048]{1,0:T(8,128)(2,1)} fusion(bf16[768,2048]{0,1:T(8,128)(2,1)} %bitcast.35, f32[767,768]{0,1:T(8,128)} %get-tuple-element.9, f32[768,768]{0,1:T(8,128)S(1)} %multiply_bitcast_fusion, f32[767,768]{0,1:T(8,128)} %get-tuple-element.8, bf16[768,2048]{1,0:T(8,128)(2,1)} %all-gather.11.cloned.1.call-done, ...), kind=kOutput, calls=%fused_computation.4 | convolution fusion | flops 4838719488 | bytes 19671552 | tf_op jit(solution)/shard_map/dot_general | solution.py:101
  264.3 31.4 %all_to_all.15 = bf16[2,384,2048]{2,1,0:T(8,128)(2,1)} all-to-all(bf16[2,384,2048]{2,1,0:T(8,128)(2,1)} %bitcast.36), channel_id=1, replica_groups=mesh['rep'=2,'fs_0'=2,'fs_1'=4,'fs_2'=4,'tp'=2] {'tp'}, dimensions={0} | all-to-all | bytes 6291456 | tf_op jit(solution)/shard_map/all_to_all | solution.py:57
  295.7 4.4 stack.2
  300.1 6.5 %all-to-all-start.1 = ((bf16[32,2048,64]{1,2,0:T(8,128)(2,1)}), bf16[32,2048,64]{1,2,0:T(8,128)(2,1)}, u32[]{:S(2)}, u32[]{:S(2)}) async-start(bf16[32,2048,64]{1,2,0:T(8,128)(2,1)} %stack.2), calls=%async_computation.1 | async-start | bytes 16777216 | tf_op jit(solution)/shard_map/all_to_all | solution.py:17
  306.6 0.0 copy-start.1
  306.6 0.0 all-gather.13.cloned.1.call-start
  306.6 3.1 convert_reduce_fusion.1
  309.7 0.5 fusion.11
  310.2 0.7 multiply_reduce_fusion.1
  310.9 1.8 multiply_convert_fusion.2
  312.8 0.0 all-gather.13.cloned.1.call-update
  312.8 176.2 %all-gather.15.cloned.1.call-done = bf16[2048,2048]{1,0:T(8,128)(2,1)} async-done(((bf16[64,2048]{1,0:T(8,128)(2,1)}), bf16[2048,2048]{1,0:T(8,128)(2,1)}) %all-gather.15.cloned.1.call-update) | async-done | bytes 8388624 | tf_op jit(solution)/shard_map/all_gather | solution.py:110
  489.0 33.0 %all-gather.13.cloned.1.call-done = bf16[768,2048]{1,0:T(8,128)(2,1)} async-done(((bf16[384,2048]{1,0:T(8,128)(2,1)}), bf16[768,2048]{1,0:T(8,128)(2,1)}) %all-gather.13.cloned.1.call-update) | async-done | bytes 3145744 | tf_op jit(solution)/shard_map/all_gather | solution.py:108
  522.1 10.0 %multiply_convert_fusion = bf16[768,2048]{1,0:T(8,128)(2,1)S(1)} fusion(bf16[768,2048]{1,0:T(8,128)(2,1)} %all-gather.13.cloned.1.call-done, bf16[2048,2048]{1,0:T(8,128)(2,1)} %all-gather.15.cloned.1.call-done), kind=kOutput, calls=%fused_computation.1 | convolution fusion | flops 6447169536 | bytes 14680064 | tf_op jit(solution)/shard_map/dot_general | solution.py:111
  532.1 0.0 all-to-all-done.1
  532.1 9.1 %convolution_convert_fusion = bf16[768,2048]{1,0:T(8,128)(2,1)S(1)} fusion(bf16[768,2048]{1,0:T(8,128)(2,1)S(1)} %multiply_convert_fusion, bf16[2048,2048]{0,1:T(8,128)(2,1)} %bitcast.10), kind=kOutput, calls=%fused_computation.3 | convolution fusion | flops 6444023808 | bytes 14680064 | tf_op jit(solution)/shard_map/dot_general | solution.py:117
  541.3 6.2 %all_to_all.16 = bf16[2,384,2048]{2,1,0:T(8,128)(2,1)S(1)} all-to-all(bf16[2,384,2048]{2,1,0:T(8,128)(2,1)S(1)} %bitcast.37), channel_id=1, replica_groups=mesh['rep'=2,'fs_0'=2,'fs_1'=4,'fs_2'=4,'tp'=2] {'tp'}, dimensions={0} | all-to-all | bytes 6291456 | tf_op jit(solution)/shard_map/all_to_all | solution.py:57
  547.5 0.7 convert_reduce_fusion
  548.2 0.7 copy-done
  548.9 0.5 fusion.12
  549.4 0.7 multiply_reduce_fusion
  550.1 1.8 multiply_convert_fusion.1
  (25 shorter events, 0.2 us)
Async XLA Ops:
  6.5 20.9 %copy-start.4 = (f32[64,768]{1,0:T(8,128)S(1)}, f32[64,768]{1,0:T(8,128)}, u32[]{:S(2)}) copy-start(f32[64,768]{1,0:T(8,128)} %param.11) | copy-start | bytes 589828
  6.5 20.9 %copy-start.5 = (f32[64,768]{1,0:T(8,128)S(1)}, f32[64,768]{1,0:T(8,128)}, u32[]{:S(2)}) copy-start(f32[64,768]{1,0:T(8,128)} %param.12) | copy-start | bytes 589828
  6.5 21.0 %copy-start.6 = (f32[64,768]{1,0:T(8,128)S(1)}, f32[64,768]{1,0:T(8,128)}, u32[]{:S(2)}) copy-start(f32[64,768]{1,0:T(8,128)} %param.13) | copy-start | bytes 589828
  6.5 21.8 %copy-start.2 = (f32[64,2048]{1,0:T(8,128)S(1)}, f32[64,2048]{1,0:T(8,128)}, u32[]{:S(2)}) copy-start(f32[64,2048]{1,0:T(8,128)} %param.17) | copy-start | bytes 1572868
  6.5 63.8 %all-gather.17.cloned.1.call-start = ((), (), s32[]{:S(2)}) async-start(), calls=%async_computation.7 | async-start | bytes 3932160 | tf_op jit(solution)/shard_map/all_gather | solution.py:39
  13.2 15.9 %copy-start.3 = (f32[2048,64]{0,1:T(8,128)S(1)}, f32[2048,64]{0,1:T(8,128)}, u32[]{:S(2)}) copy-start(f32[2048,64]{0,1:T(8,128)} %param.18) | copy-start | bytes 1572868
  26.6 2.6 copy-start.9
  26.6 61.0 %all-gather.11.cloned.1.call-start = ((), (), s32[]{:S(2)}) async-start(), calls=%async_computation.4 | async-start | bytes 4718592 | tf_op jit(solution)/shard_map/all_gather | solution.py:89
  27.4 209.8 %all-gather.9.cloned.1.call-start = ((), (), s32[]{:S(2)}) async-start(), calls=%async_computation.3 | async-start | bytes 9732096 | tf_op jit(solution)/shard_map/all_gather | solution.py:27
  28.3 460.7 %all-gather.15.cloned.1.call-start = ((), (), s32[]{:S(2)}) async-start(), calls=%async_computation.6 | async-start | bytes 8650752 | tf_op jit(solution)/shard_map/all_gather | solution.py:110
  237.2 5.7 %copy-start.10 = (bf16[768,2048]{1,0:T(8,128)(2,1)S(1)}, bf16[768,2048]{1,0:T(8,128)(2,1)}, u32[]{:S(2)}) copy-start(bf16[768,2048]{1,0:T(8,128)(2,1)} %all-gather.11.cloned.1.call-done) | copy-start | bytes 9437188
  300.1 232.0 %all-to-all-start.1 = ((bf16[32,2048,64]{1,2,0:T(8,128)(2,1)}), bf16[32,2048,64]{1,2,0:T(8,128)(2,1)}, u32[]{:S(2)}, u32[]{:S(2)}) async-start(bf16[32,2048,64]{1,2,0:T(8,128)(2,1)} %stack.2), calls=%async_computation.1 | async-start | bytes 16777216 | tf_op jit(solution)/shard_map/all_to_all | solution.py:17
  306.6 3.1 copy-start.1
  306.6 215.5 %all-gather.13.cloned.1.call-start = ((), (), s32[]{:S(2)}) async-start(), calls=%async_computation.5 | async-start | bytes 4718592 | tf_op jit(solution)/shard_map/all_gather | solution.py:108
  310.2 0.7 copy-start.7
  547.5 1.4 copy-start
  549.4 0.7 copy-start.8
Sparse Core Ops, SparseCore 0:
  26.8 43.5 all-gather.16
  72.0 15.6 all-gather.10
  89.3 147.8 all-gather.8
  238.7 250.2 all-gather.14
  490.5 31.4 all-gather.12
